TPU v7x, 32 devices: a whole 2x2x4 slice. The times are simulated.
32 devices in a mesh: sp: 8 (over z, y), tp: 4 (over x, core).
Axes of the slice: x: 2, y: 2, z: 4, core: 2. Of those that a mesh axis runs over, the one named last changes fastest.
Arguments:
- expert_input: bfloat16 [3072, 2048], P('sp'), may hold values from -6 to 6
- cotangent: bfloat16 [3072, 2048], P('sp'), may hold values from -6 to 6
- routes: int32 [3072, 2], P('sp'), may hold values from 0 to 7, all different within a row; in each aligned block of 384 rows (0 to 383, 384 to 767, ...) at most 144 rows name the same one
- route_weight: float32 [3072, 2], P('sp'), may hold values from 0.2 to 2.5
- expert_gate: bfloat16 [8, 2048, 1024], P('sp', None, 'tp'), may hold values from -0.125 to 0.125
- expert_up: bfloat16 [8, 2048, 1024], P('sp', None, 'tp'), may hold values from -0.125 to 0.125
- expert_down: bfloat16 [8, 1024, 2048], P('sp', 'tp'), may hold values from -0.1875 to 0.1875
- conv_out: bfloat16 [3072, 1024], P('sp', 'tp'), may hold values from -14 to 14
- conv_value: bfloat16 [3072, 1024], P('sp', 'tp'), may hold values from -6 to 6
- conv_gate: bfloat16 [3072, 1024], P('sp', 'tp'), may hold values from -6 to 6
- conv_taps: float32 [31, 1024], P(None, 'tp'), may hold values from -1 to 1
- norm_gain: float32 [1024], P('tp'), may hold values from 0.1 to 1.9
- norm_bias: float32 [1024], P('tp'), may hold values from -3 to 3
- out_weight: bfloat16 [1024, 2048], P('tp'), may hold values from -0.1875 to 0.1875
Outputs:
- gate_grad: float32 [8, 2048, 1024], P('sp', None, 'tp')
- up_grad: float32 [8, 2048, 1024], P('sp', None, 'tp')
- down_grad: float32 [8, 1024, 2048], P('sp', 'tp')
- resid_grad: bfloat16 [3072, 2048], P('sp')
- out_weight_grad: float32 [1024, 2048], P('tp', 'sp')
- value_grad: bfloat16 [3072, 1024], P('sp', 'tp')
- gate_in_grad: bfloat16 [3072, 1024], P('sp', 'tp')
Inputs may be any that keep to these rules, and one draw needn't show every extreme that they name: `routes`: each token names 2 different experts. In each aligned block of 384 tokens no expert is named by more than 144 tokens, and in every draw some block has an expert named by exactly 144 tokens.
All inputs are finite; a program needn't handle non-finite values.
Results may differ from a plain program's by a relative error of at most 0.018.
Values may be sent and summed in bfloat16 or wider, within the bound.
A program may use at most 128 MiB of HBM per device.

v0:
```python
import functools

import jax
import jax.numpy as jnp
from jax import lax
from jax.experimental import pallas as pl
from jax.experimental.pallas import tpu as pltpu
from jax.sharding import PartitionSpec as P

norm_eps = 1e-06
MESH = pl.DeviceIdType.MESH
bf16 = jnp.bfloat16
f32 = jnp.float32


def doublings(count):
    steps, step = [], 1
    while step < count:
        steps.append(step)
        step *= 2
    return steps


def block_order(count):
    low, high, order = 1, count - 1, []
    while low <= high:
        order.append(high)
        if low < high:
            order.append(low)
        low, high = low + 1, high - 1
    return order


def greet(me_s, me_t, sp, tp):
    barrier = pltpu.get_barrier_semaphore()
    peers = [(me_s ^ d, me_t) for d in range(1, sp)] + [(me_s, me_t ^ q) for q in range(1, tp)]
    for peer in peers:
        pl.semaphore_signal(barrier, inc=1, device_id=peer, device_id_type=MESH)
    pl.semaphore_wait(barrier, len(peers))


def remote(source, target, send_sem, recv_sem, peer):
    return pltpu.make_async_remote_copy(
        src_ref=source,
        dst_ref=target,
        send_sem=send_sem,
        recv_sem=recv_sem,
        device_id=peer,
        device_id_type=MESH,
    )


def two_rows(first, second):
    lane = lax.broadcasted_iota(jnp.int32, (first.shape[0], 128), 1)
    tile = jnp.where(lane == 0, first, jnp.where(lane == 1, second, 0.0))
    return tile.T[:8]


def share_sums(held_ref, send_sem, recv_sem, me_s, me_t, tp):
    copies = [
        remote(
            held_ref.at[0], held_ref.at[q], send_sem.at[q], recv_sem.at[q], (me_s, me_t ^ q)
        )
        for q in range(1, tp)
    ]
    for copy in copies:
        copy.start()
    return copies


def summed(held_ref, copies):
    value = held_ref[0]
    for q, copy in enumerate(copies, 1):
        copy.wait_recv()
        value = value + held_ref[q]
    return value


def expert_kernel(sp, tp, *refs):
    (rows_ref, cots_ref, gate_ref, up_ref, down_ref, pick_ref, cot_ref, conv_ref) = refs[:8]
    (resid_ref, gate_out, up_out, down_out, stats_out) = refs[8:13]
    refs = refs[2:]
    (in_ref, hid_ref, gpre_ref, upre_ref, part_ref, got_ref, sums_ref, fin_ref) = refs[11:19]
    (back_ref, acc_ref, own_sem, send_sem, recv_sem, got_send, got_recv) = refs[19:26]
    (back_send, back_recv, join_send, join_recv, stat_ref, stat_send, stat_recv) = refs[26:]
    me_s, me_t = lax.axis_index("sp"), lax.axis_index("tp")
    share = cot_ref.shape[-1]
    local_exp, capacity = rows_ref.shape[1:3]
    steps = doublings(tp)
    depth = len(steps)
    order = [0] + block_order(sp)
    sent = (rows_ref, cots_ref)
    slot, sent_slot = {}, {}
    for k, m in enumerate(steps):
        for q in range(0, tp, 2 * m):
            slot[k, q] = len(slot)
            if k:
                sent_slot[k, q ^ m] = len(sent_slot)

    def cols(q):
        return pl.ds(pl.multiple_of((me_t ^ q) * share, share), share)

    greet(me_s, me_t, sp, tp)
    copies = {}

    for d in order:
        for a in range(2):
            if d:
                copy = remote(
                    sent[a].at[me_s ^ d],
                    in_ref.at[a, me_s, :, :, cols(0)],
                    send_sem.at[0, a, d],
                    recv_sem.at[0, a, d],
                    (me_s ^ d, me_t),
                )
            else:
                copy = pltpu.make_async_copy(
                    sent[a].at[me_s], in_ref.at[a, me_s, :, :, cols(0)], own_sem.at[a]
                )
            copy.start()
            copies[0, a, d] = copy

    def forward(a, d, q, m):
        place = in_ref.at[a, me_s ^ d, :, :, cols(q)]
        source = sent[a].at[me_s] if d == 0 and q == 0 else place
        copy = remote(
            source,
            place,
            send_sem.at[q ^ m, a, d],
            recv_sem.at[q ^ m, a, d],
            (me_s, me_t ^ m),
        )
        copy.start()
        copies[q ^ m, a, d] = copy

    def spread(d):
        for a in range(2):
            if d:
                copies[0, a, d].wait_recv()
            for m in reversed(steps):
                forward(a, d, 0, m)

    def relay(d):
        for a in range(2):
            for low in reversed(steps[1:]):
                for q in range(low, tp, 2 * low):
                    copies[q, a, d].wait_recv()
                    for m in reversed(steps):
                        if m < low:
                            forward(a, d, q, m)

    def give(k, q, d, source):
        m = steps[k]
        place = slot[k, q ^ m]
        copy = remote(
            source,
            got_ref.at[place, me_s ^ d],
            got_send.at[place, d],
            got_recv.at[place, d],
            (me_s, me_t ^ m),
        )
        copy.start()
        copies["got", k, q ^ m, d] = copy

    def dot(left, right, contract):
        return lax.dot_general(left, right, (contract, ((), ())), preferred_element_type=f32)

    def compute(d):
        for a in range(2):
            for q in range(1, tp, 2):
                copies[q, a, d].wait_recv()
            if d == 0:
                copies[0, a, d].wait()
        at = me_s ^ d
        for e in range(local_exp):
            slot_rows, slot_cots = in_ref[0, at, e], in_ref[1, at, e]
            pre_gate = dot(slot_rows, gate_ref[e], ((1,), (0,)))
            pre_up = dot(slot_rows, up_ref[e], ((1,), (0,)))
            hidden_grad = dot(slot_cots, down_ref[e], ((1,), (1,)))
            gate_sig = jax.nn.sigmoid(pre_gate)
            gate_act = pre_gate * gate_sig
            hid_ref[e, at] = (gate_act * pre_up).astype(bf16)
            gate_pre = (
                hidden_grad * pre_up * gate_sig * (1.0 + pre_gate * (1.0 - gate_sig))
            ).astype(bf16)
            up_pre = (hidden_grad * gate_act).astype(bf16)
            gpre_ref[e, at] = gate_pre
            upre_ref[e, at] = up_pre
            part = dot(gate_pre, gate_ref[e], ((1,), (1,)))
            part = part + dot(up_pre, up_ref[e], ((1,), (1,)))
            part_ref[at, e] = part.astype(bf16)
        for q in range(1, tp, 2):
            give(0, q, d, part_ref.at[at, :, :, cols(q)])

    def total(k, q, d):
        value = part_ref[me_s ^ d, :, :, cols(q)].astype(f32)
        for j in range(k):
            value = value + got_ref[slot[j, q], me_s ^ d].astype(f32)
        return value.astype(bf16)

    def reduce(k, d):
        for q in range(0, tp, 2 * steps[k - 1]):
            copies["got", k - 1, q, d].wait_recv()
        if k < depth:
            m = steps[k]
            for q in range(m, tp, 2 * m):
                held = sums_ref.at[sent_slot[k, q], me_s ^ d]
                held[...] = total(k, q, d)
                give(k, q, d, held)
        elif d:
            fin_ref[me_s ^ d] = total(k, 0, d)
            copy = remote(
                fin_ref.at[me_s ^ d],
                back_ref.at[me_s],
                back_send.at[d],
                back_recv.at[d],
                (me_s ^ d, me_t),
            )
            copy.start()
            copies["back", d] = copy
        else:
            back_ref[me_s] = total(k, 0, d)

    conv_vals = conv_ref[...].astype(f32)
    stat_ref[0] = two_rows(
        jnp.sum(conv_vals, axis=1, keepdims=True),
        jnp.sum(conv_vals * conv_vals, axis=1, keepdims=True),
    )

    plan = [(0, spread), (1, relay), (2, compute)]
    plan += [(2 + k, functools.partial(reduce, k)) for k in range(1, depth + 1)]
    stat_copies = []
    for i in range(len(order) + plan[-1][0]):
        if i == 1:
            stat_copies = share_sums(stat_ref, stat_send, stat_recv, me_s, me_t, tp)
        for lag, act in plan:
            if 0 <= i - lag < len(order):
                act(order[i - lag])

    def weight_grad(e, left, right, out):
        if capacity % 16 == 0:
            whole = lambda value: value.reshape(sp * capacity, value.shape[-1])
            out[e] = dot(whole(left(slice(None))), whole(right(slice(None))), ((0,), (0,)))
        else:
            out[e] = jnp.zeros(out.shape[1:], f32)

            @pl.loop(0, sp)
            def _(at):
                out[e] += dot(left(at), right(at), ((0,), (0,)))

    for e in range(local_exp):
        weight_grad(e, lambda at: in_ref[0, at, e], lambda at: gpre_ref[e, at], gate_out)
        weight_grad(e, lambda at: in_ref[0, at, e], lambda at: upre_ref[e, at], up_out)
        weight_grad(e, lambda at: hid_ref[e, at], lambda at: in_ref[1, at, e], down_out)

    acc_ref[...] = cot_ref[...].astype(f32)
    for d in order:
        if d:
            copies["back", d].wait_recv()
        for e in range(local_exp):
            acc_ref[...] += dot(pick_ref[me_s ^ d, e], back_ref[me_s ^ d, e], ((1,), (0,)))
    resid_ref[:, cols(0)] = acc_ref[...].astype(bf16)

    def join(q, m):
        place = resid_ref.at[:, cols(q)]
        copy = remote(
            place, place, join_send.at[q ^ m], join_recv.at[q ^ m], (me_s, me_t ^ m)
        )
        copy.start()
        copies["join", q ^ m] = copy

    for m in reversed(steps):
        join(0, m)
    for low in reversed(steps[1:]):
        for q in range(low, tp, 2 * low):
            copies["join", q].wait_recv()
            for m in reversed(steps):
                if m < low:
                    join(q, m)
    for q in range(1, tp, 2):
        copies["join", q].wait_recv()
    stats_out[...] = summed(stat_ref, stat_copies)
    for copy in stat_copies:
        copy.wait_send()
    for key, copy in copies.items():
        if not (key[0] == 0 and key[-1] == 0):
            copy.wait_send()


def run_experts(send_rows, send_cots, gate, up, down, picks, own_cot, conv_out, sp, tp):
    _, local_exp, capacity, share = send_rows.shape
    width, hidden = gate.shape[1:]
    tok_rows = own_cot.shape[0]
    vmem = pl.BlockSpec(memory_space=pltpu.VMEM)
    spare = max(1, tp // 2 - 1)
    part = (sp, local_exp, capacity, share)
    kept = (local_exp, sp, capacity, hidden)
    dma = pltpu.SemaphoreType.DMA
    return pl.pallas_call(
        functools.partial(expert_kernel, sp, tp),
        out_shape=(
            jax.ShapeDtypeStruct((tok_rows, width), bf16),
            jax.ShapeDtypeStruct(gate.shape, f32),
            jax.ShapeDtypeStruct(up.shape, f32),
            jax.ShapeDtypeStruct(down.shape, f32),
            jax.ShapeDtypeStruct((8, tok_rows), f32),
        ),
        in_specs=[vmem] * 8,
        out_specs=(vmem,) * 5,
        scratch_shapes=[
            pltpu.VMEM((2, sp, local_exp, capacity, width), bf16),
            pltpu.VMEM(kept, bf16),
            pltpu.VMEM(kept, bf16),
            pltpu.VMEM(kept, bf16),
            pltpu.VMEM((sp, local_exp, capacity, width), bf16),
            pltpu.VMEM((tp - 1, *part), bf16),
            pltpu.VMEM((spare, *part), bf16),
            pltpu.VMEM(part, bf16),
            pltpu.VMEM(part, bf16),
            pltpu.VMEM((tok_rows, share), f32),
            dma((2,)),
            dma((tp, 2, sp)),
            dma((tp, 2, sp)),
            dma((tp - 1, sp)),
            dma((tp - 1, sp)),
            dma((sp,)),
            dma((sp,)),
            dma((tp,)),
            dma((tp,)),
            pltpu.VMEM((tp, 8, tok_rows), f32),
            dma((tp,)),
            dma((tp,)),
        ],
        compiler_params=pltpu.CompilerParams(
            collective_id=0, has_side_effects=True, vmem_limit_bytes=62 * 1024 * 1024
        ),
    )(send_rows, send_cots, gate, up, down, picks, own_cot, conv_out)


def conv_kernel(sp, tp, *refs):
    (resid_ref, stats_ref, conv_ref, value_ref, gate_ref, taps_ref) = refs[:6]
    (gain_ref, bias_ref, weight_ref) = refs[6:9]
    (weight_out, value_out, gate_out) = refs[9:12]
    (proj_ref, low_ref, near_ref, sum_ref, far_ref, ext_ref, halo_ref, stat_ref) = refs[12:20]
    (near_send, near_recv, far_send, far_recv) = refs[20:24]
    (halo_send, halo_recv, stat_send, stat_recv) = refs[24:]
    me_s, me_t = lax.axis_index("sp"), lax.axis_index("tp")
    tok_rows, own_channels = conv_ref.shape
    channels = own_channels * tp
    taps_count = taps_ref.shape[0]
    halo_rows = halo_ref.shape[0]
    pairs = min(2, sp)
    order = [d for d in block_order(sp) if d % pairs == 0] + [0]

    greet(me_s, me_t, sp, tp)

    totals = stats_ref[...].T / channels
    row_mean = totals[:, 0:1]
    row_rstd = lax.rsqrt(totals[:, 1:2] - row_mean * row_mean + norm_eps)
    normed = (conv_ref[...].astype(f32) - row_mean) * row_rstd
    norm_pre = normed * gain_ref[...] + bias_ref[...]
    norm_sig = jax.nn.sigmoid(norm_pre)
    conv_act = (norm_pre * norm_sig).astype(bf16)
    projected = lax.dot_general(
        resid_ref[...], conv_act, (((0,), (0,)), ((), ())), preferred_element_type=f32
    )
    proj_ref[...] = projected.reshape(proj_ref.shape)
    low_ref[...] = proj_ref[...].astype(bf16)

    near, far = {}, {}
    if pairs == 2:
        for d in order:
            near[d] = remote(
                low_ref.at[me_s ^ 1 ^ d],
                near_ref.at[d // 2],
                near_send.at[d // 2],
                near_recv.at[d // 2],
                (me_s ^ 1, me_t),
            )
            near[d].start()

    def pass_on(d):
        near[d].wait_recv()
        if d:
            sum_ref[d // 2] = (proj_ref[me_s ^ d] + near_ref[d // 2].astype(f32)).astype(bf16)
            far[d] = remote(
                sum_ref.at[d // 2],
                far_ref.at[d // 2],
                far_send.at[d // 2],
                far_recv.at[d // 2],
                (me_s ^ d, me_t),
            )
            far[d].start()

    mix_grad = lax.dot_general(
        resid_ref[...], weight_ref[...], (((1,), (1,)), ((), ())), preferred_element_type=f32
    )
    norm_grad = mix_grad * norm_sig * (1.0 + norm_pre * (1.0 - norm_sig)) * gain_ref[...]
    stat_ref[0] = two_rows(
        jnp.sum(norm_grad, axis=1, keepdims=True),
        jnp.sum(norm_grad * normed, axis=1, keepdims=True),
    )
    stat_copies = share_sums(stat_ref, stat_send, stat_recv, me_s, me_t, tp)
    means = summed(stat_ref, stat_copies).T / channels
    ext_ref[0:tok_rows, :] = row_rstd * (norm_grad - means[:, 0:1] - normed * means[:, 1:2])
    halo = remote(
        ext_ref.at[0:halo_rows, :],
        halo_ref,
        halo_send,
        halo_recv,
        (lax.rem(me_s + sp - 1, sp), me_t),
    )
    halo.start()

    chunk = 64 if tok_rows % 64 == 0 else tok_rows
    starts = list(range(0, tok_rows, chunk))

    def convolve(start):
        glu_grad = jnp.zeros((chunk, own_channels), f32)
        for lag_index in range(taps_count):
            begin = start + taps_count - 1 - lag_index
            glu_grad = glu_grad + taps_ref[lag_index, :][None, :] * ext_ref[
                begin : begin + chunk, :
            ]
        at = slice(start, start + chunk)
        gate_sig = jax.nn.sigmoid(gate_ref[at, :].astype(f32))
        value_out[at, :] = (glu_grad * gate_sig).astype(bf16)
        gate_out[at, :] = (
            glu_grad * value_ref[at, :].astype(f32) * gate_sig * (1.0 - gate_sig)
        ).astype(bf16)

    early = [start for start in starts if start + chunk + taps_count - 1 <= tok_rows]
    for i in range(max(len(order), len(early))):
        if i < len(order) and pairs == 2:
            pass_on(order[i])
        if i < len(early):
            convolve(early[i])
    halo.wait_recv()
    ext_ref[tok_rows : tok_rows + halo_rows, :] = jnp.where(me_s == sp - 1, 0.0, halo_ref[...])
    for start in starts[len(early) :]:
        convolve(start)

    total = proj_ref[me_s]
    if pairs == 2:
        total = total + near_ref[0].astype(f32)
    for d in order[:-1]:
        far[d].wait_recv()
        total = total + far_ref[d // 2].astype(f32)
    weight_out[...] = total
    for copy in [halo, *stat_copies, *near.values(), *far.values()]:
        copy.wait_send()


def run_conv(resid, stats, conv, value, gate, taps, gain, bias, weight, sp, tp):
    tok_rows, own_channels = conv.shape
    share = resid.shape[1] // sp
    vmem = pl.BlockSpec(memory_space=pltpu.VMEM)
    dma = pltpu.SemaphoreType.DMA
    half = max(1, sp // 2)
    halo_rows = -(-(taps.shape[0] - 1) // 8) * 8
    return pl.pallas_call(
        functools.partial(conv_kernel, sp, tp),
        out_shape=(
            jax.ShapeDtypeStruct((share, own_channels), f32),
            jax.ShapeDtypeStruct(conv.shape, bf16),
            jax.ShapeDtypeStruct(conv.shape, bf16),
        ),
        in_specs=[vmem] * 9,
        out_specs=(vmem,) * 3,
        scratch_shapes=[
            pltpu.VMEM((sp, share, own_channels), f32),
            pltpu.VMEM((sp, share, own_channels), bf16),
            pltpu.VMEM((half, share, own_channels), bf16),
            pltpu.VMEM((half, share, own_channels), bf16),
            pltpu.VMEM((half, share, own_channels), bf16),
            pltpu.VMEM((tok_rows + halo_rows, own_channels), f32),
            pltpu.VMEM((halo_rows, own_channels), f32),
            pltpu.VMEM((tp, 8, tok_rows), f32),
            dma((half,)),
            dma((half,)),
            dma((half,)),
            dma((half,)),
            dma(()),
            dma(()),
            dma((tp,)),
            dma((tp,)),
        ],
        compiler_params=pltpu.CompilerParams(
            collective_id=1, has_side_effects=True, vmem_limit_bytes=40 * 1024 * 1024
        ),
    )(resid, stats, conv, value, gate, taps, gain, bias, weight)


def on_device(
    expert_input,
    cotangent,
    routes,
    route_weight,
    expert_gate,
    expert_up,
    expert_down,
    conv_out,
    conv_value,
    conv_gate,
    conv_taps,
    norm_gain,
    norm_bias,
    out_weight,
):
    sp_count = lax.axis_size("sp")
    tp_count = lax.axis_size("tp")
    tok_rows, model_width = expert_input.shape
    share_cols = model_width // tp_count
    top_count = routes.shape[1]
    local_exp = expert_gate.shape[0]
    experts = local_exp * sp_count
    capacity = 3 * top_count * tok_rows // (2 * experts)
    named = routes[:, :, None] == jnp.arange(experts, dtype=jnp.int32)
    token_at = jnp.arange(tok_rows, dtype=jnp.int32)
    earlier = (token_at[:, None] > token_at[None, :]).astype(jnp.bfloat16)
    before = jnp.dot(
        earlier, jnp.any(named, axis=1).astype(jnp.bfloat16), preferred_element_type=jnp.float32
    )
    slot_rank = jnp.sum(jnp.where(named, before[:, None, :], 0.0), axis=2).astype(jnp.int32)
    target = routes * capacity + slot_rank
    blocks = (sp_count, local_exp, tok_rows, capacity)
    slot_at = (
        lax.broadcasted_iota(jnp.int32, blocks, 0) * local_exp
        + lax.broadcasted_iota(jnp.int32, blocks, 1)
    ) * capacity + lax.broadcasted_iota(jnp.int32, blocks, 3)
    pick = [
        (target[:, k][None, None, :, None] == slot_at).astype(jnp.bfloat16) for k in range(top_count)
    ]
    picks = sum(pick[1:], pick[0])
    share_at = lax.axis_index("tp") * share_cols
    own_in = lax.dynamic_slice_in_dim(expert_input, share_at, share_cols, 1)
    own_cot = lax.dynamic_slice_in_dim(cotangent, share_at, share_cols, 1)

    def chosen(which, values):
        return jnp.einsum("setr,td->serd", which, values, preferred_element_type=jnp.float32)

    send_rows = chosen(picks, own_in).astype(jnp.bfloat16)
    send_cot = sum(
        chosen(
            pick[k],
            (own_cot.astype(jnp.float32) * route_weight[:, k][:, None]).astype(jnp.bfloat16),
        )
        for k in range(top_count)
    ).astype(jnp.bfloat16)
    resid_grad, gate_grad, up_grad, down_grad, row_stats = run_experts(
        send_rows,
        send_cot,
        expert_gate,
        expert_up,
        expert_down,
        picks,
        own_cot,
        conv_out,
        sp_count,
        tp_count,
    )
    projected, value_grad, gate_in_grad = run_conv(
        resid_grad,
        row_stats,
        conv_out,
        conv_value,
        conv_gate,
        conv_taps,
        norm_gain[None, :],
        norm_bias[None, :],
        out_weight,
        sp_count,
        tp_count,
    )
    out_weight_grad = projected.T
    return (gate_grad, up_grad, down_grad, resid_grad, out_weight_grad, value_grad, gate_in_grad)


def solution(mesh):
    return jax.shard_map(
        on_device,
        mesh=mesh,
        in_specs=(
            P("sp", None),
            P("sp", None),
            P("sp", None),
            P("sp", None),
            P("sp", None, "tp"),
            P("sp", None, "tp"),
            P("sp", "tp", None),
            P("sp", "tp"),
            P("sp", "tp"),
            P("sp", "tp"),
            P(None, "tp"),
            P("tp"),
            P("tp"),
            P("tp", None),
        ),
        out_specs=(
            P("sp", None, "tp"),
            P("sp", None, "tp"),
            P("sp", "tp", None),
            P("sp", None),
            P("tp", "sp"),
            P("sp", "tp"),
            P("sp", "tp"),
        ),
        check_vma=False,
    )
```

profile of v0, /device:TPU:24, one launch (start us, length us, event | category | flops | bytes accessed | tf_op | source)
XLA Modules:
  0.0 167.7 jit_solution(13384439705195022738)
XLA Ops:
  0.6 0.0 copy-start
  0.7 0.8 fusion.40
  1.5 0.8 slice_reduce_fusion.2
  2.2 0.1 fusion.31
  2.4 0.8 select_reduce_fusion
  3.1 0.7 convert_add_fusion
  3.9 1.0 constant_dynamic-slice_fusion.refs_6_
  4.9 0.0 copy-done
  4.9 0.0 copy-start.11
  4.9 1.9 %fusion.15.refs_0_ = bf16[8,1,144,512]{3,2,1,0:T(8,128)(2,1)} fusion(s32[384]{0:T(512)S(1)} %get-tuple-element.40, s32[8]{0:T(128)S(1)} %iota_multiply_fusion, s32[384]{0:T(512)S(1)} %get-tuple-element.39, bf16[384,2048]{1,0:T(8,128)(2,1)S(1)} %copy-done, s32[]{:T(128)S(6)} %select_n.9), kind=kOutput, calls=%fused_computation.15 | convolution fusion | flops 457555968 | bytes 1577476 | tf_op jit(solution)/shard_map/setr,td->serd/dot_general | solution.py:540
  6.8 1.8 %fusion.12.refs_5_ = bf16[8,1,384,144]{3,2,1,0:T(8,128)(2,1)} fusion(s32[384]{0:T(512)S(1)} %get-tuple-element.40, s32[8]{0:T(128)S(1)} %iota_multiply_fusion, s32[384]{0:T(512)S(1)} %get-tuple-element.39), kind=kLoop, calls=%fused_computation.13 | loop fusion | flops 3981312 | bytes 887840 | tf_op jit(solution)/shard_map/add | solution.py:534
  8.5 0.9 fusion.6
  9.4 0.0 copy-done.11
  9.4 1.9 %fusion.16.refs_1_ = bf16[8,1,144,512]{3,2,1,0:T(8,128)(2,1)} fusion(f32[8,144,512]{2,1,0:T(8,128)S(1)} %fusion.6, s32[384]{0:T(512)S(1)} %get-tuple-element.40, s32[8]{0:T(128)S(1)} %iota_multiply_fusion, bf16[384,512]{1,0:T(8,128)(2,1)S(1)} %constant_dynamic-slice_fusion.refs_6_, f32[384]{0:T(512)S(1)} %get-tuple-element.37), kind=kOutput, calls=%fused_computation.16 | convolution fusion | flops 455639040 | bytes 3935264 | tf_op jit(solution)/shard_map/setr,td->serd/dot_general | solution.py:540
  11.3 0.0 copy-start.10
  11.3 115.9 %shard_map.189 = (bf16[384,2048]{1,0:T(8,128)(2,1)}, f32[1,2048,256]{2,1,0:T(8,128)}, f32[1,2048,256]{2,1,0:T(8,128)}, f32[1,256,2048]{2,1,0:T(8,128)}, f32[8,384]{1,0:T(8,128)}) custom-call(bf16[8,1,144,512]{3,2,1,0:T(8,128)(2,1)} %fusion.15.refs_0_, bf16[8,1,144,512]{3,2,1,0:T(8,128)(2,1)} %fusion.16.refs_1_, bf16[1,2048,256]{2,1,0:T(8,128)(2,1)} %refs_2_.2, ...), custom_call_target="tpu_custom_call" | custom-call | tf_op jit(solution)/shard_map/pallas_call | solution.py:299
  127.2 0.0 copy-done.4
  127.2 0.0 copy-done.5
  127.3 1.4 copy-done.1
  128.7 1.2 copy-done.3
  129.9 0.9 copy-done.6
  130.8 0.7 copy-done.8
  131.5 25.1 %shard_map.190 = (f32[256,256]{1,0:T(8,128)S(1)}, bf16[384,256]{1,0:T(8,128)(2,1)S(1)}, bf16[384,256]{1,0:T(8,128)(2,1)S(1)}) custom-call(bf16[384,2048]{1,0:T(8,128)(2,1)S(1)} %copy-done.1, f32[8,384]{1,0:T(8,128)S(1)} %copy-done.8, bf16[384,256]{1,0:T(8,128)(2,1)S(1)} %copy-done.4, bf16[384,256]{1,0:T(8,128)(2,1)S(1)} %copy-done.5, ...), custom_call_target="tpu_custom_call" | custom-call | tf_op jit(solution)/shard_map/pallas_call | solution.py:461
  156.6 0.8 copy.24
  157.4 3.2 %copy.31 = f32[1,2048,256]{2,1,0:T(8,128)} copy(f32[1,2048,256]{2,1,0:T(8,128)} %get-tuple-element.48) | data formatting | bytes 4194304
  160.6 1.3 copy.32
  162.0 1.0 copy-done.12
  163.0 1.3 copy.33
  164.3 0.8 copy-done.2
  165.2 1.1 copy.34
  166.3 0.7 copy.35
  167.0 0.7 copy.36
  (17 shorter events, 0.1 us)
Async XLA Ops:
  0.6 4.3 %copy-start = (bf16[384,2048]{1,0:T(8,128)(2,1)S(1)}, bf16[384,2048]{1,0:T(8,128)(2,1)}, u32[]{:S(2)}) copy-start(bf16[384,2048]{1,0:T(8,128)(2,1)} %param.14) | copy-start | bytes 4718596
  4.9 4.5 %copy-start.11 = (bf16[384,512]{1,0:T(8,128)(2,1)}, bf16[384,512]{1,0:T(8,128)(2,1)S(1)}, u32[]{:S(2)}) copy-start(bf16[384,512]{1,0:T(8,128)(2,1)S(1)} %constant_dynamic-slice_fusion.refs_6_) | copy-start | bytes 1179652
  11.3 115.9 %copy-start.4 = (bf16[384,256]{1,0:T(8,128)(2,1)S(1)}, bf16[384,256]{1,0:T(8,128)(2,1)}, u32[]{:S(2)}) copy-start(bf16[384,256]{1,0:T(8,128)(2,1)} %refs_2_.3) | copy-start | bytes 589828
  11.3 115.9 %copy-start.5 = (bf16[384,256]{1,0:T(8,128)(2,1)S(1)}, bf16[384,256]{1,0:T(8,128)(2,1)}, u32[]{:S(2)}) copy-start(bf16[384,256]{1,0:T(8,128)(2,1)} %refs_3_.3) | copy-start | bytes 589828
  11.3 115.9 %copy-start.7 = (f32[31,256]{1,0:T(8,128)S(1)}, f32[31,256]{1,0:T(8,128)}, u32[]{:S(2)}) copy-start(f32[31,256]{1,0:T(8,128)} %refs_5_.1) | copy-start | bytes 95236
  11.3 115.9 %copy-start.9 = (f32[256]{0:T(256)S(1)}, f32[256]{0:T(256)}, u32[]{:S(2)}) copy-start(f32[256]{0:T(256)} %param.25) | copy-start | bytes 3076
  11.3 115.9 %copy-start.10 = (f32[256]{0:T(256)S(1)}, f32[256]{0:T(256)}, u32[]{:S(2)}) copy-start(f32[256]{0:T(256)} %param.26) | copy-start | bytes 3076
  127.2 1.4 copy-start.1
  128.7 1.2 copy-start.3
  129.9 0.9 copy-start.6
  130.8 0.7 copy-start.8
  157.4 3.2 %copy-start.13 = (f32[1,2048,256]{2,1,0:T(8,128)S(1)}, f32[1,2048,256]{2,1,0:T(8,128)}, u32[]{:S(2)}) copy-start(f32[1,2048,256]{2,1,0:T(8,128)} %get-tuple-element.49) | copy-start | bytes 6291460
  160.6 2.3 %copy-start.12 = (f32[1,256,2048]{2,1,0:T(8,128)S(1)}, f32[1,256,2048]{2,1,0:T(8,128)}, u32[]{:S(2)}) copy-start(f32[1,256,2048]{2,1,0:T(8,128)} %get-tuple-element.50) | copy-start | bytes 6291460
  163.0 2.2 %copy-start.2 = (bf16[384,2048]{1,0:T(8,128)(2,1)S(1)}, bf16[384,2048]{1,0:T(8,128)(2,1)}, u32[]{:S(2)}) copy-start(bf16[384,2048]{1,0:T(8,128)(2,1)} %get-tuple-element.51.refs_0_) | copy-start | bytes 4718596
where the time goes:
time: 171 us; the launch traced here: 168 us
  Pallas kernels  141 us (82%)
  local copies, waits for them, and re-layouts  17.2 us (10%)
  matrix products  4.73 us (3%)
  other arithmetic  4.05 us (2%)
    pallas_call x1, Pallas kernels, run_experts(): pl.pallas_call(functools.partial(expert_kernel, sp, tp), out_shape=(jax.S...  116 us
    pallas_call x1, Pallas kernels, run_conv(): pl.pallas_call(functools.partial(conv_kernel, sp, tp), out_shape=(jax.Sha...  25.1 us
    unnamed x35, local copies, waits for them, and re-layouts  15.3 us
    dot_general x3, matrix products, chosen(): jnp.einsum('setr,td->serd', which, values, preferred_element_type=jnp.flo...  4.6 us

commit v1 on v0

v1 whole, which is shorter than its diff:
```python
import functools

import jax
import jax.numpy as jnp
from jax import lax
from jax.experimental import pallas as pl
from jax.experimental.pallas import tpu as pltpu
from jax.sharding import PartitionSpec as P

norm_eps = 1e-06
MESH = pl.DeviceIdType.MESH
bf16 = jnp.bfloat16
f32 = jnp.float32


def doublings(count):
    steps, step = [], 1
    while step < count:
        steps.append(step)
        step *= 2
    return steps


def remote(source, target, send_sem, recv_sem, peer):
    return pltpu.make_async_remote_copy(
        src_ref=source,
        dst_ref=target,
        send_sem=send_sem,
        recv_sem=recv_sem,
        device_id=peer,
        device_id_type=MESH,
    )


def two_rows(first, second):
    lane = lax.broadcasted_iota(jnp.int32, (first.shape[0], 128), 1)
    tile = jnp.where(lane == 0, first, jnp.where(lane == 1, second, 0.0))
    return tile.T[:8]


def share_sums(held_ref, send_sem, recv_sem, me_s, me_t, tp):
    copies = [
        remote(
            held_ref.at[0], held_ref.at[q], send_sem.at[q], recv_sem.at[q], (me_s, me_t ^ q)
        )
        for q in range(1, tp)
    ]
    for copy in copies:
        copy.start()
    return copies


def summed(held_ref, copies):
    value = held_ref[0]
    for q, copy in enumerate(copies, 1):
        copy.wait_recv()
        value = value + held_ref[q]
    return value


def peers_of(me_s, me_t, sp, tp):
    return [(me_s ^ d, me_t) for d in range(1, sp)] + [(me_s, me_t ^ q) for q in range(1, tp)]


def greet(peers):
    barrier = pltpu.get_barrier_semaphore()
    for peer in peers:
        pl.semaphore_signal(barrier, inc=1, device_id=peer, device_id_type=MESH)
    return barrier


def near_blocks(sp):
    return min(4, max(1, sp // 2))


def send_order(sp):
    close = list(range(1, near_blocks(sp)))
    apart = list(range(near_blocks(sp), sp))
    order = []
    for i in range(max(len(close), len(apart))):
        order += close[i : i + 1] + apart[i : i + 1]
    return order


def dot(left, right, contract):
    return lax.dot_general(left, right, (contract, ((), ())), preferred_element_type=f32)


def step_kernel(sp, tp, *refs):
    (routes_ref, weights_ref, gain_ref, bias_ref) = refs[:4]
    sources = refs[4:14]
    (resid_ref, gate_out, up_out, down_out) = refs[14:18]
    (weight_out, value_out, glu_out) = refs[18:21]
    loaded = refs[21:31]
    (x_ref, cot_ref, conv_ref, gate_ref, up_ref) = loaded[:5]
    (down_ref, mixer_ref, value_ref, sluice_ref, taps_ref) = loaded[5:]
    (load_sem, pick_ref, packet_ref, in_ref, hid_ref, pre_ref, part_ref, got_ref) = refs[31:39]
    (back_ref, acc_ref, second_ref, send_sem, recv_sem) = refs[39:44]
    (got_send, got_recv, back_send, back_recv, join_send, join_recv) = refs[44:50]
    (stat_ref, stat_send, stat_recv, mean_ref, mean_send, mean_recv) = refs[50:56]
    (normed_ref, slope_ref, act_ref, mix_ref) = refs[56:60]
    (proj_ref, low_ref, near_ref, sum_ref, far_ref, ext_ref, halo_ref) = refs[60:67]
    (near_send, near_recv, far_send, far_recv, halo_send, halo_recv) = refs[67:]

    me_s, me_t = lax.axis_index("sp"), lax.axis_index("tp")
    tok_rows, width = x_ref.shape
    top_count = routes_ref.shape[0]
    local_exp, _, hidden = gate_ref.shape
    capacity = in_ref.shape[3]
    share = width // tp
    steps = doublings(tp)
    depth = len(steps)
    order = send_order(sp)
    close = near_blocks(sp)
    slot = {}
    for k, m in enumerate(steps):
        for q in range(0, tp, 2 * m):
            slot[k, q] = len(slot)

    def cols(q):
        return pl.ds(pl.multiple_of((me_t ^ q) * share, share), share)

    peers = peers_of(me_s, me_t, sp, tp)
    barrier = greet(peers)
    loads = [
        pltpu.make_async_copy(source, target, load_sem.at[i])
        for i, (source, target) in enumerate(zip(sources, loaded))
    ]
    for copy in loads:
        copy.start()

    experts = sp * local_exp
    routes = routes_ref[...]
    route = [routes[k : k + 1, :] for k in range(top_count)]
    expert_at = lax.broadcasted_iota(jnp.int32, (experts, tok_rows), 0)
    chosen = [route[k] == expert_at for k in range(top_count)]
    named = sum(jnp.where(hit, 1.0, 0.0) for hit in chosen).astype(bf16)
    grid = (tok_rows, tok_rows)
    earlier = jnp.where(
        lax.broadcasted_iota(jnp.int32, grid, 0) < lax.broadcasted_iota(jnp.int32, grid, 1),
        1.0,
        0.0,
    ).astype(bf16)
    before = dot(named, earlier, ((1,), (0,)))
    target = []
    for k in range(top_count):
        rank = jnp.sum(jnp.where(chosen[k], before, 0.0), axis=0, keepdims=True)
        target.append(route[k] * capacity + rank.astype(jnp.int32))
    slot_at = lax.broadcasted_iota(jnp.int32, (capacity, tok_rows), 0)

    loads[0].wait()
    loads[1].wait()
    pl.semaphore_wait(barrier, len(peers))
    copies = {}

    def packet(d, quarters, place):
        for e in range(local_exp):
            base = ((me_s ^ d) * local_exp + e) * capacity
            hits = [target[k] == slot_at + base for k in range(top_count)]
            pick = sum(jnp.where(hit, 1.0, 0.0) for hit in hits).astype(bf16)
            pick_ref[d, e] = pick
            scale = sum(
                jnp.sum(
                    jnp.where(hits[k], weights_ref[k : k + 1, :], 0.0), axis=1, keepdims=True
                )
                for k in range(top_count)
            )
            for q in quarters:
                rows = dot(pick, x_ref[:, cols(q)], ((1,), (0,)))
                cots = dot(pick, cot_ref[:, cols(q)], ((1,), (0,))) * scale
                place(q, 0, e)[...] = rows.astype(bf16)
                place(q, 1, e)[...] = cots.astype(bf16)

    def arriving(d):
        return list(range(0, tp, 2)) if d < close else [0]

    def held_packet(d, q):
        return second_ref.at[d, q // 2 - 1] if q else packet_ref.at[d]

    for d in order:
        packet(d, arriving(d), lambda q, a, e: held_packet(d, q).at[a, e])
        for q in arriving(d):
            copy = remote(
                held_packet(d, q),
                in_ref.at[me_s, :, :, :, cols(q)],
                send_sem.at[q, d],
                recv_sem.at[q, d],
                (me_s ^ d, me_t),
            )
            copy.start()
            copies[q, d] = copy

    def forward(d, q, m):
        place = in_ref.at[me_s ^ d, :, :, :, cols(q)]
        copy = remote(
            place, place, send_sem.at[q ^ m, d], recv_sem.at[q ^ m, d], (me_s, me_t ^ m)
        )
        copy.start()
        copies[q ^ m, d] = copy

    def spread(d):
        if d < close:
            for q in range(0, tp, 2):
                copies[q, d].wait_recv()
                if tp > 1:
                    forward(d, q, 1)
        else:
            copies[0, d].wait_recv()
            for m in reversed(steps):
                forward(d, 0, m)

    def relay(d):
        if d >= close:
            for low in reversed(steps[1:]):
                for q in range(low, tp, 2 * low):
                    copies[q, d].wait_recv()
                    for m in reversed(steps):
                        if m < low:
                            forward(d, q, m)

    def give(k, q, d, source):
        m = steps[k]
        place = slot[k, q ^ m]
        copy = remote(
            source,
            got_ref.at[place, me_s ^ d],
            got_send.at[place, d],
            got_recv.at[place, d],
            (me_s, me_t ^ m),
        )
        copy.start()
        copies["got", k, q ^ m, d] = copy

    def compute(d):
        if d:
            for q in range(1, tp, 2):
                copies[q, d].wait_recv()
        at = me_s ^ d
        for e in range(local_exp):
            slot_rows, slot_cots = in_ref[at, 0, e], in_ref[at, 1, e]
            pre_gate = dot(slot_rows, gate_ref[e], ((1,), (0,)))
            pre_up = dot(slot_rows, up_ref[e], ((1,), (0,)))
            hidden_grad = dot(slot_cots, down_ref[e], ((1,), (1,)))
            gate_sig = jax.nn.sigmoid(pre_gate)
            gate_act = pre_gate * gate_sig
            hid_ref[e, at] = (gate_act * pre_up).astype(bf16)
            gate_pre = (
                hidden_grad * pre_up * gate_sig * (1.0 + pre_gate * (1.0 - gate_sig))
            ).astype(bf16)
            up_pre = (hidden_grad * gate_act).astype(bf16)
            pre_ref[e, at, :, 0:hidden] = gate_pre
            pre_ref[e, at, :, hidden : 2 * hidden] = up_pre
            part = dot(gate_pre, gate_ref[e], ((1,), (1,)))
            part = part + dot(up_pre, up_ref[e], ((1,), (1,)))
            part_ref[at, e] = part.astype(bf16)
        for q in range(1, tp, 2):
            give(0, q, d, part_ref.at[at, :, :, cols(q)])

    def total(k, q, d):
        value = part_ref[me_s ^ d, :, :, cols(q)].astype(f32)
        for j in range(k):
            value = value + got_ref[slot[j, q], me_s ^ d].astype(f32)
        return value.astype(bf16)

    def reduce(k, d):
        for q in range(0, tp, 2 * steps[k - 1]):
            copies["got", k - 1, q, d].wait_recv()
        if k < depth:
            m = steps[k]
            for q in range(m, tp, 2 * m):
                held = part_ref.at[me_s ^ d, :, :, cols(q)]
                held[...] = total(k, q, d)
                give(k, q, d, held)
        elif d:
            held = part_ref.at[me_s ^ d, :, :, cols(0)]
            held[...] = total(k, 0, d)
            copy = remote(
                held,
                back_ref.at[me_s],
                back_send.at[d],
                back_recv.at[d],
                (me_s ^ d, me_t),
            )
            copy.start()
            copies["back", d] = copy
        else:
            back_ref[me_s] = total(k, 0, d)

    loads[2].wait()
    conv_vals = conv_ref[...].astype(f32)
    stat_ref[0] = two_rows(
        jnp.sum(conv_vals, axis=1, keepdims=True),
        jnp.sum(conv_vals * conv_vals, axis=1, keepdims=True),
    )
    stat_copies = share_sums(stat_ref, stat_send, stat_recv, me_s, me_t, tp)
    packet(0, range(tp), lambda q, a, e: in_ref.at[me_s, a, e, :, cols(q)])
    for copy in loads[3:6]:
        copy.wait()
    compute(0)

    channels = conv_ref.shape[1] * tp
    totals = summed(stat_ref, stat_copies).T / channels
    row_mean = totals[:, 0:1]
    row_var = jnp.maximum(totals[:, 1:2] - row_mean * row_mean, 0.0)
    row_rstd = lax.rsqrt(row_var + norm_eps)
    normed = (conv_vals - row_mean) * row_rstd
    norm_pre = normed * gain_ref[...] + bias_ref[...]
    norm_sig = jax.nn.sigmoid(norm_pre)
    normed_ref[...] = normed
    act_ref[...] = (norm_pre * norm_sig).astype(bf16)
    slope_ref[...] = norm_sig * (1.0 + norm_pre * (1.0 - norm_sig)) * gain_ref[...]

    for k in range(1, depth + 1):
        reduce(k, 0)

    plan = [(0, spread), (1, relay), (2, compute)]
    plan += [(2 + k, functools.partial(reduce, k)) for k in range(1, depth + 1)]
    for i in range(len(order) + plan[-1][0]):
        for lag, act in plan:
            if 0 <= i - lag < len(order):
                act(order[i - lag])

    def rows_grad(e, left, right, store, clear):
        if capacity % 16 == 0:
            whole = lambda value: value.reshape(sp * capacity, value.shape[-1])
            store(dot(whole(left(slice(None))), whole(right(slice(None))), ((0,), (0,))))
        else:
            clear()

            @pl.loop(0, sp)
            def _(at):
                store(dot(left(at), right(at), ((0,), (0,))))

    for e in range(local_exp):
        adds = capacity % 16 != 0

        def put(ref, value):
            ref[e] = ref[e] + value if adds else value

        def put_both(both):
            put(gate_out, both[:, 0:hidden])
            put(up_out, both[:, hidden : 2 * hidden])

        def zero(*outs):
            for out in outs:
                out[e] = jnp.zeros(out.shape[1:], f32)

        rows_grad(
            e,
            lambda at: in_ref[at, 0, e],
            lambda at: pre_ref[e, at],
            put_both,
            functools.partial(zero, gate_out, up_out),
        )
        rows_grad(
            e,
            lambda at: hid_ref[e, at],
            lambda at: in_ref[at, 1, e],
            functools.partial(put, down_out),
            functools.partial(zero, down_out),
        )

    for copy in loads[6:]:
        copy.wait()
    acc_ref[...] = cot_ref[:, cols(0)].astype(f32)
    for d in [0] + order:
        if d:
            copies["back", d].wait_recv()
        for e in range(local_exp):
            acc_ref[...] += dot(pick_ref[d, e], back_ref[me_s ^ d, e], ((0,), (0,)))
    resid_ref[:, cols(0)] = acc_ref[...].astype(bf16)

    def join(q, m):
        place = resid_ref.at[:, cols(q)]
        copy = remote(
            place, place, join_send.at[q ^ m], join_recv.at[q ^ m], (me_s, me_t ^ m)
        )
        copy.start()
        copies["join", q ^ m] = copy

    for m in reversed(steps):
        join(0, m)

    pairs = sp // 2
    per_quarter = pairs // tp
    own_pair, side = lax.div(me_s, 2), lax.rem(me_s, 2)
    feats = proj_ref.shape[2]
    own_channels = conv_ref.shape[1]

    def pair_copies(p):
        near = remote(
            low_ref.at[p], near_ref.at[p], near_send.at[p], near_recv.at[p], (me_s ^ 1, me_t)
        )
        far = remote(
            sum_ref.at[p],
            far_ref.at[own_pair],
            far_send.at[p],
            far_recv.at[own_pair],
            (2 * p + side, me_t),
        )
        return near, far

    def pairs_in(q):
        return [(me_t ^ q) * per_quarter + j for j in range(per_quarter)]

    def project(q):
        quarter = resid_ref[:, cols(q)]
        projected = dot(quarter, act_ref[...], ((0,), (0,)))
        for j, p in enumerate(pairs_in(q)):
            start = 2 * j * feats
            proj_ref[p] = projected[start : start + 2 * feats].reshape(2, feats, own_channels)
            low_ref[p] = proj_ref[p, 1 - side].astype(bf16)
            pair_copies(p)[0].start()
        mixed = dot(quarter, mixer_ref[:, cols(q)], ((1,), (1,)))
        if q == 0:
            mix_ref[...] = mixed
        else:
            mix_ref[...] += mixed

    def pass_on(q):
        for p in pairs_in(q):
            near, far = pair_copies(p)
            near.wait_recv()

            @pl.when(p != own_pair)
            def _():
                sum_ref[p] = (proj_ref[p, side] + near_ref[p].astype(f32)).astype(bf16)
                far.start()

    forwards = {}
    for low in reversed(steps[1:]):
        for q in range(low, tp, 2 * low):
            forwards[q] = [m for m in reversed(steps) if m < low]
    ready = [0] + [q for q in range(1, tp) if q not in forwards and q in (1,)]
    ready += [q for q in range(1, tp) if q not in ready and q in forwards]
    ready += [q for q in range(1, tp) if q not in ready]
    for i, q in enumerate(ready):
        if q:
            copies["join", q].wait_recv()
            for m in forwards.get(q, []):
                join(q, m)
        project(q)
        if 1 <= i < len(ready) - 1:
            pass_on(ready[i - 1])

    norm_grad = mix_ref[...] * slope_ref[...]
    mean_ref[0] = two_rows(
        jnp.sum(norm_grad, axis=1, keepdims=True),
        jnp.sum(norm_grad * normed_ref[...], axis=1, keepdims=True),
    )
    mean_copies = share_sums(mean_ref, mean_send, mean_recv, me_s, me_t, tp)
    pass_on(ready[-2])
    means = summed(mean_ref, mean_copies).T / channels
    ext_ref[0:tok_rows, :] = row_rstd * (
        norm_grad - means[:, 0:1] - normed_ref[...] * means[:, 1:2]
    )
    halo_rows = halo_ref.shape[0]
    halo = remote(
        ext_ref.at[0:halo_rows, :],
        halo_ref,
        halo_send,
        halo_recv,
        (lax.rem(me_s + sp - 1, sp), me_t),
    )
    halo.start()
    pass_on(ready[-1])

    taps_count = taps_ref.shape[0]
    chunk = 64 if tok_rows % 64 == 0 else tok_rows

    def convolve(start):
        glu_grad = jnp.zeros((chunk, own_channels), f32)
        for lag_index in range(taps_count):
            begin = start + taps_count - 1 - lag_index
            glu_grad = glu_grad + taps_ref[lag_index, :][None, :] * ext_ref[
                begin : begin + chunk, :
            ]
        at = slice(start, start + chunk)
        gate_sig = jax.nn.sigmoid(sluice_ref[at, :].astype(f32))
        value_out[at, :] = (glu_grad * gate_sig).astype(bf16)
        glu_out[at, :] = (
            glu_grad * value_ref[at, :].astype(f32) * gate_sig * (1.0 - gate_sig)
        ).astype(bf16)

    starts = list(range(0, tok_rows, chunk))
    early = [start for start in starts if start + chunk + taps_count - 1 <= tok_rows]
    for start in early:
        convolve(start)
    halo.wait_recv()
    ext_ref[tok_rows : tok_rows + halo_rows, :] = jnp.where(me_s == sp - 1, 0.0, halo_ref[...])
    for start in starts[len(early) :]:
        convolve(start)

    total_grad = proj_ref[own_pair, side] + near_ref[own_pair].astype(f32)
    for x in range(1, pairs):
        other = own_pair ^ x
        remote(
            sum_ref.at[other],
            far_ref.at[other],
            far_send.at[other],
            far_recv.at[other],
            (2 * other + side, me_t),
        ).wait_recv()
        total_grad = total_grad + far_ref[other].astype(f32)
    weight_out[...] = total_grad.T

    for x in range(pairs):
        near, far = pair_copies(own_pair ^ x)
        near.wait_send()
        if x:
            far.wait_send()
    for copy in [halo, *stat_copies, *mean_copies, *copies.values()]:
        copy.wait_send()


def store_kernel(*refs):
    count = len(refs) // 2
    moves = [
        pltpu.make_async_copy(refs[i], refs[count + i], refs[-1].at[i]) for i in range(count)
    ]
    for move in moves:
        move.start()
    for move in moves:
        move.wait()


def run_step(routes, weights, gain, bias, big, sp, tp):
    x, _, conv, gate, up, down = big[:6]
    taps = big[9]
    tok_rows, width = x.shape
    own_channels = conv.shape[1]
    local_exp, _, hidden = gate.shape
    top_count = routes.shape[0]
    capacity = 3 * top_count * tok_rows // (2 * local_exp * sp)
    share = width // tp
    feats = width // sp
    pairs = sp // 2
    halo_rows = -(-(taps.shape[0] - 1) // 8) * 8
    vmem = pl.BlockSpec(memory_space=pltpu.VMEM)
    hbm = pl.BlockSpec(memory_space=pltpu.HBM)
    part = (sp, local_exp, capacity, share)
    kept = (local_exp, sp, capacity)
    rows = (tok_rows, own_channels)
    piece = (pairs, feats, own_channels)
    dma = pltpu.SemaphoreType.DMA
    outs = (
        jax.ShapeDtypeStruct((tok_rows, width), bf16),
        jax.ShapeDtypeStruct(gate.shape, f32),
        jax.ShapeDtypeStruct(up.shape, f32),
        jax.ShapeDtypeStruct(down.shape, f32),
        jax.ShapeDtypeStruct((own_channels, feats), f32),
        jax.ShapeDtypeStruct(rows, bf16),
        jax.ShapeDtypeStruct(rows, bf16),
    )
    results = pl.pallas_call(
        functools.partial(step_kernel, sp, tp),
        out_shape=tuple(pltpu.VMEM(out.shape, out.dtype) for out in outs),
        in_specs=[vmem] * 4 + [hbm] * len(big),
        out_specs=(vmem,) * len(outs),
        scratch_shapes=[
            *[pltpu.VMEM(array.shape, array.dtype) for array in big],
            dma((len(big),)),
            pltpu.VMEM((sp, local_exp, capacity, tok_rows), bf16),
            pltpu.VMEM((sp, 2, local_exp, capacity, share), bf16),
            pltpu.VMEM((sp, 2, local_exp, capacity, width), bf16),
            pltpu.VMEM((*kept, hidden), bf16),
            pltpu.VMEM((*kept, 2 * hidden), bf16),
            pltpu.VMEM((sp, local_exp, capacity, width), bf16),
            pltpu.VMEM((tp - 1, *part), bf16),
            pltpu.VMEM(part, bf16),
            pltpu.VMEM((tok_rows, share), f32),
            pltpu.VMEM((near_blocks(sp), max(1, tp // 2 - 1), 2, local_exp, capacity, share), bf16),
            dma((tp, sp)),
            dma((tp, sp)),
            dma((tp - 1, sp)),
            dma((tp - 1, sp)),
            dma((sp,)),
            dma((sp,)),
            dma((tp,)),
            dma((tp,)),
            pltpu.VMEM((tp, 8, tok_rows), f32),
            dma((tp,)),
            dma((tp,)),
            pltpu.VMEM((tp, 8, tok_rows), f32),
            dma((tp,)),
            dma((tp,)),
            pltpu.VMEM(rows, f32),
            pltpu.VMEM(rows, f32),
            pltpu.VMEM(rows, bf16),
            pltpu.VMEM(rows, f32),
            pltpu.VMEM((pairs, 2, feats, own_channels), f32),
            pltpu.VMEM(piece, bf16),
            pltpu.VMEM(piece, bf16),
            pltpu.VMEM(piece, bf16),
            pltpu.VMEM(piece, bf16),
            pltpu.VMEM((tok_rows + halo_rows, own_channels), f32),
            pltpu.VMEM((halo_rows, own_channels), f32),
            dma((pairs,)),
            dma((pairs,)),
            dma((pairs,)),
            dma((pairs,)),
            dma(()),
            dma(()),
        ],
        compiler_params=pltpu.CompilerParams(
            collective_id=0, has_side_effects=True, vmem_limit_bytes=55 * 1024 * 1024
        ),
    )(routes, weights, gain, bias, *[pltpu.with_memory_space_constraint(a, pltpu.HBM) for a in big])
    return pl.pallas_call(
        store_kernel,
        out_shape=outs,
        in_specs=[vmem] * len(outs),
        out_specs=(hbm,) * len(outs),
        scratch_shapes=[dma((len(outs),))],
        compiler_params=pltpu.CompilerParams(vmem_limit_bytes=4 * 1024 * 1024),
    )(*[pltpu.with_memory_space_constraint(a, pltpu.VMEM) for a in results])


def on_device(
    expert_input,
    cotangent,
    routes,
    route_weight,
    expert_gate,
    expert_up,
    expert_down,
    conv_out,
    conv_value,
    conv_gate,
    conv_taps,
    norm_gain,
    norm_bias,
    out_weight,
):
    big = (
        expert_input,
        cotangent,
        conv_out,
        expert_gate,
        expert_up,
        expert_down,
        out_weight,
        conv_value,
        conv_gate,
        conv_taps,
    )
    resid_grad, gate_grad, up_grad, down_grad, out_weight_grad, value_grad, gate_in_grad = run_step(
        routes.T,
        route_weight.T,
        norm_gain[None, :],
        norm_bias[None, :],
        big,
        lax.axis_size("sp"),
        lax.axis_size("tp"),
    )
    return (gate_grad, up_grad, down_grad, resid_grad, out_weight_grad, value_grad, gate_in_grad)


def solution(mesh):
    return jax.shard_map(
        on_device,
        mesh=mesh,
        in_specs=(
            P("sp", None),
            P("sp", None),
            P("sp", None),
            P("sp", None),
            P("sp", None, "tp"),
            P("sp", None, "tp"),
            P("sp", "tp", None),
            P("sp", "tp"),
            P("sp", "tp"),
            P("sp", "tp"),
            P(None, "tp"),
            P("tp"),
            P("tp"),
            P("tp", None),
        ),
        out_specs=(
            P("sp", None, "tp"),
            P("sp", None, "tp"),
            P("sp", "tp", None),
            P("sp", None),
            P("tp", "sp"),
            P("sp", "tp"),
            P("sp", "tp"),
        ),
        check_vma=False,
    )
```

time: 171 us -> 130 us (0.76); the launches traced: 168 us -> 129 us
  local copies, waits for them, and re-layouts: 17.2 us -> 0 us
  Pallas kernels: 141 us -> 128 us
  matrix products: 4.73 us -> 0 us
  other arithmetic: 4.05 us -> 0 us
    unnamed x35 -> x0, local copies, waits for them, and re-layouts: 15.3 us -> none
    pallas_call x2, Pallas kernels: 141 us -> 128 us  [the longest x1 125 us: run_step(): pl.pallas_call(functools.partial(step_kernel, sp, tp), out_shape=tuple((p...]
    dot_general x4 -> x0, matrix products: 4.73 us -> none  [the longest x3 4.6 us: chosen(): jnp.einsum('setr,td->serd', which, values, preferred_element_type=jnp.flo...]
    add x2 -> x0, other arithmetic: 2.47 us -> none  [the longest x1 1.78 us: on_device(): picks = sum(pick[1:], pick[0])]
where the time goes in v1:
time: 130 us; the launch traced here: 129 us
  Pallas kernels  128 us (98%)
    pallas_call x1, Pallas kernels, run_step(): pl.pallas_call(functools.partial(step_kernel, sp, tp), out_shape=tuple((p...  125 us
    pallas_call x1, Pallas kernels, run_step(): pl.pallas_call(store_kernel, out_shape=outs, in_specs=[vmem] * len(outs),...  3.41 us

profile of v1, /device:TPU:24, one launch (start us, length us, event | category | flops | bytes accessed | tf_op | source)
XLA Modules:
  0.0 128.9 jit_solution(10980380883667873602)
XLA Ops:
  0.6 124.7 %shard_map.189 = (bf16[384,2048]{1,0:T(8,128)(2,1)S(1)}, f32[1,2048,256]{2,1,0:T(8,128)S(1)}, f32[1,2048,256]{2,1,0:T(8,128)S(1)}, f32[1,256,2048]{2,1,0:T(8,128...) custom-call(s32[2,384]{1,0:T(2,128)} %bitcast.4, f32[2,384]{1,0:T(2,128)} %bitcast.5, ...), custom_call_target="tpu_custom_call" | custom-call | tf_op jit(solution)/shard_map/pallas_call | solution.py:555
  125.3 3.4 %shard_map.190 = (bf16[384,2048]{1,0:T(8,128)(2,1)}, f32[1,2048,256]{2,1,0:T(8,128)}, f32[1,2048,256]{2,1,0:T(8,128)}, f32[1,256,2048]{2,1,0:T(8,128)}, f32[256,...) custom-call(bf16[384,2048]{1,0:T(8,128)(2,1)S(1)} %get-tuple-element.21.refs_0_, ...), custom_call_target="tpu_custom_call" | custom-call | tf_op jit(solution)/shard_map/pallas_call | solution.py:609

commit v2 on v1

--- a/solution.py
+++ b/solution.py
@@ -73,13 +73,24 @@
     return min(4, max(1, sp // 2))
 
 
+def apart_blocks(sp):
+    return list(range(max(1, sp // 2), sp))
+
+
+def close_blocks(sp):
+    return list(range(1, max(1, sp // 2)))
+
+
 def send_order(sp):
-    close = list(range(1, near_blocks(sp)))
-    apart = list(range(near_blocks(sp), sp))
-    order = []
-    for i in range(max(len(close), len(apart))):
-        order += close[i : i + 1] + apart[i : i + 1]
-    return order
+    apart, close = apart_blocks(sp), close_blocks(sp)
+    half = len(apart) // 2
+    apart = [apart[i // 2 + (i % 2) * half] for i in range(2 * half)] + apart[2 * half :]
+    return close[:1] + apart + close[1:][::-1]
+
+
+def work_order(sp):
+    apart, close = apart_blocks(sp), close_blocks(sp)
+    return apart[:2] + close[:1] + apart[2:3] + close[2:] + apart[3:] + close[1:2]
 
 
 def dot(left, right, contract):
@@ -91,26 +102,37 @@
     sources = refs[4:14]
     (resid_ref, gate_out, up_out, down_out) = refs[14:18]
     (weight_out, value_out, glu_out) = refs[18:21]
-    loaded = refs[21:31]
-    (x_ref, cot_ref, conv_ref, gate_ref, up_ref) = loaded[:5]
-    (down_ref, mixer_ref, value_ref, sluice_ref, taps_ref) = loaded[5:]
-    (load_sem, pick_ref, packet_ref, in_ref, hid_ref, pre_ref, part_ref, got_ref) = refs[31:39]
-    (back_ref, acc_ref, second_ref, send_sem, recv_sem) = refs[39:44]
-    (got_send, got_recv, back_send, back_recv, join_send, join_recv) = refs[44:50]
-    (stat_ref, stat_send, stat_recv, mean_ref, mean_send, mean_recv) = refs[50:56]
-    (normed_ref, slope_ref, act_ref, mix_ref) = refs[56:60]
-    (proj_ref, low_ref, near_ref, sum_ref, far_ref, ext_ref, halo_ref) = refs[60:67]
-    (near_send, near_recv, far_send, far_recv, halo_send, halo_recv) = refs[67:]
+    loaded = refs[21:30]
+    (x_ref, cot_ref, conv_ref, wide_ref) = loaded[:4]
+    (down_ref, mixer_ref, value_ref, sluice_ref, taps_ref) = loaded[4:]
+    (load_sem, pick_ref, packet_ref, in_ref, hid_ref, pre_ref, part_ref, got_ref) = refs[30:38]
+    (back_ref, acc_ref, second_ref, send_sem, recv_sem) = refs[38:43]
+    (got_send, got_recv, back_send, back_recv, join_send, join_recv) = refs[43:49]
+    (stat_ref, stat_send, stat_recv, mean_ref, mean_send, mean_recv) = refs[49:55]
+    (normed_ref, slope_ref, act_ref, mix_ref) = refs[55:59]
+    (proj_ref, low_ref, near_ref, sum_ref, far_ref, ext_ref, halo_ref) = refs[59:66]
+    (near_send, near_recv, far_send, far_recv, halo_send, halo_recv) = refs[66:]
 
     me_s, me_t = lax.axis_index("sp"), lax.axis_index("tp")
     tok_rows, width = x_ref.shape
     top_count = routes_ref.shape[0]
-    local_exp, _, hidden = gate_ref.shape
+    local_exp, _, hidden = gate_out.shape
+    places = [x_ref, cot_ref, conv_ref]
+    places += [wide_ref.at[:, :, 0:hidden], wide_ref.at[:, :, hidden : 2 * hidden]]
+    places += loaded[4:]
     capacity = in_ref.shape[3]
     share = width // tp
     steps = doublings(tp)
     depth = len(steps)
-    order = send_order(sp)
+    order = work_order(sp)
+    quarter_size = max(1, sp // 4)
+    row = lax.div(me_s, quarter_size)
+    at_end = (row == 0) | (row == sp // quarter_size - 1)
+    flip = jnp.where(at_end, quarter_size if sp >= 4 else 0, 0)
+
+    def turned(d):
+        return d ^ flip if d >= max(1, sp // 2) else d
+
     close = near_blocks(sp)
     slot = {}
     for k, m in enumerate(steps):
@@ -124,7 +146,7 @@
     barrier = greet(peers)
     loads = [
         pltpu.make_async_copy(source, target, load_sem.at[i])
-        for i, (source, target) in enumerate(zip(sources, loaded))
+        for i, (source, target) in enumerate(zip(sources, places))
     ]
     for copy in loads:
         copy.start()
@@ -177,55 +199,66 @@
     def held_packet(d, q):
         return second_ref.at[d, q // 2 - 1] if q else packet_ref.at[d]
 
-    for d in order:
+    for d in send_order(sp):
         packet(d, arriving(d), lambda q, a, e: held_packet(d, q).at[a, e])
         for q in arriving(d):
-            copy = remote(
-                held_packet(d, q),
-                in_ref.at[me_s, :, :, :, cols(q)],
-                send_sem.at[q, d],
-                recv_sem.at[q, d],
-                (me_s ^ d, me_t),
-            )
-            copy.start()
-            copies[q, d] = copy
-
-    def forward(d, q, m):
-        place = in_ref.at[me_s ^ d, :, :, :, cols(q)]
+            for a in range(2):
+                copy = remote(
+                    held_packet(d, q).at[a],
+                    in_ref.at[me_s, a, :, :, cols(q)],
+                    send_sem.at[q, a, d],
+                    recv_sem.at[q, a, d],
+                    (me_s ^ d, me_t),
+                )
+                copy.start()
+                copies[q, a, d] = copy
+
+    def arrival(q, a, d):
+        place = in_ref.at[me_s ^ turned(d), a, :, :, cols(q)]
+        sems = (send_sem.at[q, a, turned(d)], recv_sem.at[q, a, turned(d)])
+        return remote(place, place, *sems, (me_s, me_t ^ max(steps, default=0)))
+
+    def forward(a, d, q, m):
+        at = turned(d)
+        place = in_ref.at[me_s ^ at, a, :, :, cols(q)]
         copy = remote(
-            place, place, send_sem.at[q ^ m, d], recv_sem.at[q ^ m, d], (me_s, me_t ^ m)
+            place,
+            place,
+            send_sem.at[q ^ m, a, at],
+            recv_sem.at[q ^ m, a, at],
+            (me_s, me_t ^ m),
         )
         copy.start()
-        copies[q ^ m, d] = copy
-
-    def spread(d):
+        copies["on", q ^ m, a, d] = copy
+
+    def spread(a, d):
         if d < close:
             for q in range(0, tp, 2):
-                copies[q, d].wait_recv()
+                arrival(q, a, d).wait_recv()
                 if tp > 1:
-                    forward(d, q, 1)
+                    forward(a, d, q, 1)
         else:
-            copies[0, d].wait_recv()
+            arrival(0, a, d).wait_recv()
             for m in reversed(steps):
-                forward(d, 0, m)
-
-    def relay(d):
+                forward(a, d, 0, m)
+
+    def relay(a, d):
         if d >= close:
             for low in reversed(steps[1:]):
                 for q in range(low, tp, 2 * low):
-                    copies[q, d].wait_recv()
+                    arrival(q, a, d).wait_recv()
                     for m in reversed(steps):
                         if m < low:
-                            forward(d, q, m)
+                            forward(a, d, q, m)
 
     def give(k, q, d, source):
         m = steps[k]
         place = slot[k, q ^ m]
         copy = remote(
             source,
-            got_ref.at[place, me_s ^ d],
-            got_send.at[place, d],
-            got_recv.at[place, d],
+            got_ref.at[place, me_s ^ turned(d)],
+            got_send.at[place, turned(d)],
+            got_recv.at[place, turned(d)],
             (me_s, me_t ^ m),
         )
         copy.start()
@@ -234,12 +267,13 @@
     def compute(d):
         if d:
             for q in range(1, tp, 2):
-                copies[q, d].wait_recv()
-        at = me_s ^ d
+                for a in range(2):
+                    arrival(q, a, d).wait_recv()
+        at = me_s ^ turned(d)
         for e in range(local_exp):
             slot_rows, slot_cots = in_ref[at, 0, e], in_ref[at, 1, e]
-            pre_gate = dot(slot_rows, gate_ref[e], ((1,), (0,)))
-            pre_up = dot(slot_rows, up_ref[e], ((1,), (0,)))
+            pre = dot(slot_rows, wide_ref[e], ((1,), (0,)))
+            pre_gate, pre_up = pre[:, 0:hidden], pre[:, hidden : 2 * hidden]
             hidden_grad = dot(slot_cots, down_ref[e], ((1,), (1,)))
             gate_sig = jax.nn.sigmoid(pre_gate)
             gate_act = pre_gate * gate_sig
@@ -250,16 +284,15 @@
             up_pre = (hidden_grad * gate_act).astype(bf16)
             pre_ref[e, at, :, 0:hidden] = gate_pre
             pre_ref[e, at, :, hidden : 2 * hidden] = up_pre
-            part = dot(gate_pre, gate_ref[e], ((1,), (1,)))
-            part = part + dot(up_pre, up_ref[e], ((1,), (1,)))
-            part_ref[at, e] = part.astype(bf16)
+            both = jnp.concatenate([gate_pre, up_pre], axis=1)
+            part_ref[at, e] = dot(both, wide_ref[e], ((1,), (1,))).astype(bf16)
         for q in range(1, tp, 2):
             give(0, q, d, part_ref.at[at, :, :, cols(q)])
 
     def total(k, q, d):
-        value = part_ref[me_s ^ d, :, :, cols(q)].astype(f32)
+        value = part_ref[me_s ^ turned(d), :, :, cols(q)].astype(f32)
         for j in range(k):
-            value = value + got_ref[slot[j, q], me_s ^ d].astype(f32)
+            value = value + got_ref[slot[j, q], me_s ^ turned(d)].astype(f32)
         return value.astype(bf16)
 
     def reduce(k, d):
@@ -268,18 +301,15 @@
         if k < depth:
             m = steps[k]
             for q in range(m, tp, 2 * m):
-                held = part_ref.at[me_s ^ d, :, :, cols(q)]
+                held = part_ref.at[me_s ^ turned(d), :, :, cols(q)]
                 held[...] = total(k, q, d)
                 give(k, q, d, held)
         elif d:
-            held = part_ref.at[me_s ^ d, :, :, cols(0)]
+            at = turned(d)
+            held = part_ref.at[me_s ^ at, :, :, cols(0)]
             held[...] = total(k, 0, d)
             copy = remote(
-                held,
-                back_ref.at[me_s],
-                back_send.at[d],
-                back_recv.at[d],
-                (me_s ^ d, me_t),
+                held, back_ref.at[me_s], back_send.at[at], back_recv.at[at], (me_s ^ at, me_t)
             )
             copy.start()
             copies["back", d] = copy
@@ -299,26 +329,36 @@
     compute(0)
 
     channels = conv_ref.shape[1] * tp
-    totals = summed(stat_ref, stat_copies).T / channels
-    row_mean = totals[:, 0:1]
-    row_var = jnp.maximum(totals[:, 1:2] - row_mean * row_mean, 0.0)
-    row_rstd = lax.rsqrt(row_var + norm_eps)
-    normed = (conv_vals - row_mean) * row_rstd
-    norm_pre = normed * gain_ref[...] + bias_ref[...]
-    norm_sig = jax.nn.sigmoid(norm_pre)
-    normed_ref[...] = normed
-    act_ref[...] = (norm_pre * norm_sig).astype(bf16)
-    slope_ref[...] = norm_sig * (1.0 + norm_pre * (1.0 - norm_sig)) * gain_ref[...]
-
-    for k in range(1, depth + 1):
-        reduce(k, 0)
-
-    plan = [(0, spread), (1, relay), (2, compute)]
-    plan += [(2 + k, functools.partial(reduce, k)) for k in range(1, depth + 1)]
-    for i in range(len(order) + plan[-1][0]):
+
+    def normalise():
+        totals = summed(stat_ref, stat_copies).T / channels
+        row_mean = totals[:, 0:1]
+        row_var = jnp.maximum(totals[:, 1:2] - row_mean * row_mean, 0.0)
+        row_rstd = lax.rsqrt(row_var + norm_eps)
+        normed = (conv_ref[...].astype(f32) - row_mean) * row_rstd
+        norm_pre = normed * gain_ref[...] + bias_ref[...]
+        norm_sig = jax.nn.sigmoid(norm_pre)
+        normed_ref[...] = normed
+        act_ref[...] = (norm_pre * norm_sig).astype(bf16)
+        slope_ref[...] = norm_sig * (1.0 + norm_pre * (1.0 - norm_sig)) * gain_ref[...]
+        return row_rstd
+
+    def rest(d):
+        for k in range(2, depth + 1):
+            reduce(k, d)
+
+    spread0, spread1 = functools.partial(spread, 0), functools.partial(spread, 1)
+    relay0, relay1 = functools.partial(relay, 0), functools.partial(relay, 1)
+    r1, r2 = functools.partial(reduce, 1), rest
+    plan = [(4, r2), (3, r1), (2, compute), (1, relay0), (1, relay1), (0, spread0), (0, spread1)]
+    for i in range(len(order) + max(lag for lag, _ in plan)):
         for lag, act in plan:
             if 0 <= i - lag < len(order):
                 act(order[i - lag])
+        if i == 1:
+            row_rstd = normalise()
+        if 1 <= i <= depth:
+            reduce(i, 0)
 
     def rows_grad(e, left, right, store, clear):
         if capacity % 16 == 0:
@@ -331,117 +371,158 @@
             def _(at):
                 store(dot(left(at), right(at), ((0,), (0,))))
 
-    for e in range(local_exp):
-        adds = capacity % 16 != 0
-
-        def put(ref, value):
-            ref[e] = ref[e] + value if adds else value
-
-        def put_both(both):
-            put(gate_out, both[:, 0:hidden])
-            put(up_out, both[:, hidden : 2 * hidden])
-
-        def zero(*outs):
-            for out in outs:
-                out[e] = jnp.zeros(out.shape[1:], f32)
-
-        rows_grad(
-            e,
-            lambda at: in_ref[at, 0, e],
-            lambda at: pre_ref[e, at],
-            put_both,
-            functools.partial(zero, gate_out, up_out),
-        )
-        rows_grad(
-            e,
-            lambda at: hid_ref[e, at],
-            lambda at: in_ref[at, 1, e],
-            functools.partial(put, down_out),
-            functools.partial(zero, down_out),
-        )
+    adds = capacity % 16 != 0
+
+    def put(ref, e, value):
+        ref[e] = ref[e] + value if adds else value
+
+    def clear(outs, e):
+        for out in outs:
+            out[e] = jnp.zeros(out.shape[1:], f32)
+
+    def input_side_grads():
+        for e in range(local_exp):
+
+            def put_both(both):
+                put(gate_out, e, both[:, 0:hidden])
+                put(up_out, e, both[:, hidden : 2 * hidden])
+
+            rows_grad(
+                e,
+                lambda at: in_ref[at, 0, e],
+                lambda at: pre_ref[e, at],
+                put_both,
+                functools.partial(clear, (gate_out, up_out), e),
+            )
+
+    def output_side_grads():
+        for e in range(local_exp):
+            rows_grad(
+                e,
+                lambda at: hid_ref[e, at],
+                lambda at: in_ref[at, 1, e],
+                functools.partial(put, down_out, e),
+                functools.partial(clear, (down_out,), e),
+            )
 
     for copy in loads[6:]:
         copy.wait()
     acc_ref[...] = cot_ref[:, cols(0)].astype(f32)
     for d in [0] + order:
         if d:
-            copies["back", d].wait_recv()
+            came = back_ref.at[me_s ^ turned(d)]
+            sems = (back_send.at[turned(d)], back_recv.at[turned(d)])
+            remote(came, came, *sems, (me_s ^ turned(d), me_t)).wait_recv()
         for e in range(local_exp):
-            acc_ref[...] += dot(pick_ref[d, e], back_ref[me_s ^ d, e], ((0,), (0,)))
+            picked = pick_ref[turned(d), e]
+            acc_ref[...] += dot(picked, back_ref[me_s ^ turned(d), e], ((0,), (0,)))
     resid_ref[:, cols(0)] = acc_ref[...].astype(bf16)
-
-    def join(q, m):
-        place = resid_ref.at[:, cols(q)]
-        copy = remote(
-            place, place, join_send.at[q ^ m], join_recv.at[q ^ m], (me_s, me_t ^ m)
-        )
-        copy.start()
-        copies["join", q ^ m] = copy
-
-    for m in reversed(steps):
-        join(0, m)
 
     pairs = sp // 2
     per_quarter = pairs // tp
     own_pair, side = lax.div(me_s, 2), lax.rem(me_s, 2)
     feats = proj_ref.shape[2]
     own_channels = conv_ref.shape[1]
-
-    def pair_copies(p):
-        near = remote(
+    pieces = 2 if per_quarter == 1 and feats % 128 == 0 else 1
+    piece_cols = share // pieces
+
+    def piece(q, h):
+        offset = (me_t ^ q) * share
+        if pieces == 2:
+            offset = offset + (side if h else 1 - side) * feats
+        return pl.ds(pl.multiple_of(offset, piece_cols), piece_cols)
+
+    def join(q, h, m):
+        place = resid_ref.at[:, piece(q, h)]
+        copy = remote(
+            place, place, join_send.at[q ^ m, h], join_recv.at[q ^ m, h], (me_s, me_t ^ m)
+        )
+        copy.start()
+        copies["join", q ^ m, h] = copy
+
+    for h in range(pieces):
+        for m in reversed(steps):
+            join(0, h, m)
+
+    def pair_near(p):
+        return remote(
             low_ref.at[p], near_ref.at[p], near_send.at[p], near_recv.at[p], (me_s ^ 1, me_t)
         )
-        far = remote(
+
+    def pair_far(p):
+        return remote(
             sum_ref.at[p],
             far_ref.at[own_pair],
             far_send.at[p],
             far_recv.at[own_pair],
             (2 * p + side, me_t),
         )
-        return near, far
 
     def pairs_in(q):
         return [(me_t ^ q) * per_quarter + j for j in range(per_quarter)]
 
-    def project(q):
-        quarter = resid_ref[:, cols(q)]
+    def project(q, h):
+        quarter = resid_ref[:, piece(q, h)]
         projected = dot(quarter, act_ref[...], ((0,), (0,)))
-        for j, p in enumerate(pairs_in(q)):
-            start = 2 * j * feats
-            proj_ref[p] = projected[start : start + 2 * feats].reshape(2, feats, own_channels)
-            low_ref[p] = proj_ref[p, 1 - side].astype(bf16)
-            pair_copies(p)[0].start()
-        mixed = dot(quarter, mixer_ref[:, cols(q)], ((1,), (1,)))
-        if q == 0:
+        if pieces == 2:
+            p = (me_t ^ q) * per_quarter
+            if h:
+                proj_ref[p, side] = projected
+            else:
+                low_ref[p] = projected.astype(bf16)
+                pair_near(p).start()
+        else:
+            for j, p in enumerate(pairs_in(q)):
+                start = 2 * j * feats
+                both = projected[start : start + 2 * feats]
+                proj_ref[p] = both.reshape(2, feats, own_channels)
+                low_ref[p] = proj_ref[p, 1 - side].astype(bf16)
+                pair_near(p).start()
+        mixed = dot(quarter, mixer_ref[:, piece(q, h)], ((1,), (1,)))
+        if q == 0 and h == 0:
             mix_ref[...] = mixed
         else:
             mix_ref[...] += mixed
 
     def pass_on(q):
         for p in pairs_in(q):
-            near, far = pair_copies(p)
-            near.wait_recv()
+            pair_near(p).wait_recv()
 
             @pl.when(p != own_pair)
             def _():
                 sum_ref[p] = (proj_ref[p, side] + near_ref[p].astype(f32)).astype(bf16)
-                far.start()
-
-    forwards = {}
+                pair_far(p).start()
+
+    onward = {}
     for low in reversed(steps[1:]):
         for q in range(low, tp, 2 * low):
-            forwards[q] = [m for m in reversed(steps) if m < low]
-    ready = [0] + [q for q in range(1, tp) if q not in forwards and q in (1,)]
-    ready += [q for q in range(1, tp) if q not in ready and q in forwards]
-    ready += [q for q in range(1, tp) if q not in ready]
-    for i, q in enumerate(ready):
-        if q:
-            copies["join", q].wait_recv()
-            for m in forwards.get(q, []):
-                join(q, m)
-        project(q)
-        if 1 <= i < len(ready) - 1:
-            pass_on(ready[i - 1])
+            onward[q] = [m for m in reversed(steps) if m < low]
+
+    def arrived(q, h):
+        copies["join", q, h].wait_recv()
+        for m in onward.get(q, []):
+            join(q, h, m)
+
+    direct = [q for q in range(1, tp) if q in steps]
+    ready = sorted(direct) + [q for q in range(1, tp) if q not in direct]
+    quick, slow = ready[:1], ready[1:]
+    for h in range(pieces):
+        project(0, h)
+    for q in quick:
+        for h in range(pieces):
+            arrived(q, h)
+            project(q, h)
+    input_side_grads()
+    for q in [0] + quick:
+        pass_on(q)
+    late = [(q, h) for h in range(pieces) for q in slow]
+    for q, h in late[:1]:
+        arrived(q, h)
+        project(q, h)
+    output_side_grads()
+    for q, h in late[1:]:
+        arrived(q, h)
+        project(q, h)
 
     norm_grad = mix_ref[...] * slope_ref[...]
     mean_ref[0] = two_rows(
@@ -449,7 +530,8 @@
         jnp.sum(norm_grad * normed_ref[...], axis=1, keepdims=True),
     )
     mean_copies = share_sums(mean_ref, mean_send, mean_recv, me_s, me_t, tp)
-    pass_on(ready[-2])
+    for q in slow:
+        pass_on(q)
     means = summed(mean_ref, mean_copies).T / channels
     ext_ref[0:tok_rows, :] = row_rstd * (
         norm_grad - means[:, 0:1] - normed_ref[...] * means[:, 1:2]
@@ -463,7 +545,6 @@
         (lax.rem(me_s + sp - 1, sp), me_t),
     )
     halo.start()
-    pass_on(ready[-1])
 
     taps_count = taps_ref.shape[0]
     chunk = 64 if tok_rows % 64 == 0 else tok_rows
@@ -505,10 +586,9 @@
     weight_out[...] = total_grad.T
 
     for x in range(pairs):
-        near, far = pair_copies(own_pair ^ x)
-        near.wait_send()
+        pair_near(own_pair ^ x).wait_send()
         if x:
-            far.wait_send()
+            pair_far(own_pair ^ x).wait_send()
     for copy in [halo, *stat_copies, *mean_copies, *copies.values()]:
         copy.wait_send()
 
@@ -558,7 +638,9 @@
         in_specs=[vmem] * 4 + [hbm] * len(big),
         out_specs=(vmem,) * len(outs),
         scratch_shapes=[
-            *[pltpu.VMEM(array.shape, array.dtype) for array in big],
+            *[pltpu.VMEM(array.shape, array.dtype) for array in big[:3]],
+            pltpu.VMEM((local_exp, width, 2 * hidden), bf16),
+            *[pltpu.VMEM(array.shape, array.dtype) for array in big[5:]],
             dma((len(big),)),
             pltpu.VMEM((sp, local_exp, capacity, tok_rows), bf16),
             pltpu.VMEM((sp, 2, local_exp, capacity, share), bf16),
@@ -570,14 +652,14 @@
             pltpu.VMEM(part, bf16),
             pltpu.VMEM((tok_rows, share), f32),
             pltpu.VMEM((near_blocks(sp), max(1, tp // 2 - 1), 2, local_exp, capacity, share), bf16),
-            dma((tp, sp)),
-            dma((tp, sp)),
+            dma((tp, 2, sp)),
+            dma((tp, 2, sp)),
             dma((tp - 1, sp)),
             dma((tp - 1, sp)),
             dma((sp,)),
             dma((sp,)),
-            dma((tp,)),
-            dma((tp,)),
+            dma((tp, 2)),
+            dma((tp, 2)),
             pltpu.VMEM((tp, 8, tok_rows), f32),
             dma((tp,)),
             dma((tp,)),

time: 130 us -> 119 us (0.915)
  Pallas kernels: 128 us -> 118 us
    pallas_call x1, Pallas kernels: 125 us -> 115 us  [run_step(): pl.pallas_call(functools.partial(step_kernel, sp, tp), out_shape=tuple((p...]
where the time goes in v2:
time: 119 us
  Pallas kernels  118 us (99%)
    pallas_call x1, Pallas kernels, run_step(): pl.pallas_call(functools.partial(step_kernel, sp, tp), out_shape=tuple((p...  115 us
    pallas_call x1, Pallas kernels, run_step(): pl.pallas_call(store_kernel, out_shape=outs, in_specs=[vmem] * len(outs),...  3.41 us

profile of v2, /device:TPU:24, one launch (start us, length us, event | category | flops | bytes accessed | tf_op | source)
XLA Modules:
  0.0 118.7 jit_solution(5250760462241737965)
XLA Ops:
  0.6 114.5 %shard_map.189 = (bf16[384,2048]{1,0:T(8,128)(2,1)S(1)}, f32[1,2048,256]{2,1,0:T(8,128)S(1)}, f32[1,2048,256]{2,1,0:T(8,128)S(1)}, f32[1,256,2048]{2,1,0:T(8,128...) custom-call(s32[2,384]{1,0:T(2,128)} %bitcast.4, f32[2,384]{1,0:T(2,128)} %bitcast.5, ...), custom_call_target="tpu_custom_call" | custom-call | tf_op jit(solution)/shard_map/pallas_call | solution.py:635
  115.2 3.4 %shard_map.190 = (bf16[384,2048]{1,0:T(8,128)(2,1)}, f32[1,2048,256]{2,1,0:T(8,128)}, f32[1,2048,256]{2,1,0:T(8,128)}, f32[1,256,2048]{2,1,0:T(8,128)}, f32[256,...) custom-call(bf16[384,2048]{1,0:T(8,128)(2,1)S(1)} %get-tuple-element.21.refs_0_, ...), custom_call_target="tpu_custom_call" | custom-call | tf_op jit(solution)/shard_map/pallas_call | solution.py:691

commit v3 on v2

--- a/solution.py
+++ b/solution.py
@@ -350,7 +350,7 @@
     spread0, spread1 = functools.partial(spread, 0), functools.partial(spread, 1)
     relay0, relay1 = functools.partial(relay, 0), functools.partial(relay, 1)
     r1, r2 = functools.partial(reduce, 1), rest
-    plan = [(4, r2), (3, r1), (2, compute), (1, relay0), (1, relay1), (0, spread0), (0, spread1)]
+    plan = [(0, spread0), (1, relay0), (0, spread1), (1, relay1), (2, r1), (1, compute), (3, r2)]
     for i in range(len(order) + max(lag for lag, _ in plan)):
         for lag, act in plan:
             if 0 <= i - lag < len(order):
@@ -515,6 +515,9 @@
     input_side_grads()
     for q in [0] + quick:
         pass_on(q)
+    sent = [key for key in copies if key[0] != "join"]
+    for key in sent:
+        copies.pop(key).wait_send()
     late = [(q, h) for h in range(pieces) for q in slow]
     for q, h in late[:1]:
         arrived(q, h)

time: 119 us -> 119 us (level)
  no operation moved by 1% of the time
where the time goes in v3:
time: 119 us; the launch traced here: 118 us
  Pallas kernels  118 us (99%)
    pallas_call x1, Pallas kernels, run_step(): pl.pallas_call(functools.partial(step_kernel, sp, tp), out_shape=tuple((p...  114 us
    pallas_call x1, Pallas kernels, run_step(): pl.pallas_call(store_kernel, out_shape=outs, in_specs=[vmem] * len(outs),...  3.41 us

profile of v3, /device:TPU:24, one launch (start us, length us, event | category | flops | bytes accessed | tf_op | source)
XLA Modules:
  0.0 118.3 jit_solution(935226816830339627)
XLA Ops:
  0.6 114.1 %shard_map.189 = (bf16[384,2048]{1,0:T(8,128)(2,1)S(1)}, f32[1,2048,256]{2,1,0:T(8,128)S(1)}, f32[1,2048,256]{2,1,0:T(8,128)S(1)}, f32[1,256,2048]{2,1,0:T(8,128...) custom-call(s32[2,384]{1,0:T(2,128)} %bitcast.4, f32[2,384]{1,0:T(2,128)} %bitcast.5, ...), custom_call_target="tpu_custom_call" | custom-call | tf_op jit(solution)/shard_map/pallas_call | solution.py:638
  114.8 3.4 %shard_map.190 = (bf16[384,2048]{1,0:T(8,128)(2,1)}, f32[1,2048,256]{2,1,0:T(8,128)}, f32[1,2048,256]{2,1,0:T(8,128)}, f32[1,256,2048]{2,1,0:T(8,128)}, f32[256,...) custom-call(bf16[384,2048]{1,0:T(8,128)(2,1)S(1)} %get-tuple-element.21.refs_0_, ...), custom_call_target="tpu_custom_call" | custom-call | tf_op jit(solution)/shard_map/pallas_call | solution.py:694
